TPU v7x, 32 devices: a whole 2x2x4 slice. The times are simulated.
32 devices in a mesh: ep: 16 (over z, y, core), tp: 2 (over x).
Axes of the slice: x: 2, y: 2, z: 4, core: 2. Of those that a mesh axis runs over, the one named last changes fastest.
Arguments:
- tokens: bfloat16 [256, 1024], P('ep', 'tp'), may hold values from -12 to 12
- input_window: bfloat16 [256, 3, 512], P('ep', None, 'tp'), may hold values from -6 to 6
- write_window: bfloat16 [256, 3, 256], P('ep', None, 'tp'), may hold values from -6 to 6
- read_window: bfloat16 [256, 3, 256], P('ep', None, 'tp'), may hold values from -6 to 6
- ssm_state: float32 [256, 8, 64, 64], P('ep', 'tp'), may hold values from -6 to 6
- norm_gain: bfloat16 [1024], replicated, may hold values from 0.099609375 to 1.8984375
- proj_gate: bfloat16 [1024, 512], P(None, 'tp'), may hold values from -0.1875 to 0.1875
- proj_input: bfloat16 [1024, 512], P(None, 'tp'), may hold values from -0.1875 to 0.1875
- proj_write: bfloat16 [1024, 256], P(None, 'tp'), may hold values from -0.1875 to 0.1875
- proj_read: bfloat16 [1024, 256], P(None, 'tp'), may hold values from -0.1875 to 0.1875
- proj_step: bfloat16 [1024, 8], replicated, may hold values from -0.1875 to 0.1875
- taps_input: bfloat16 [4, 512], P(None, 'tp'), may hold values from -3 to 3
- taps_write: bfloat16 [4, 256], P(None, 'tp'), may hold values from -3 to 3
- taps_read: bfloat16 [4, 256], P(None, 'tp'), may hold values from -3 to 3
- step_bias: float32 [8], replicated, may hold values from -2.5 to 0.5
- decay_rate: float32 [8], replicated, may hold values from 0.02 to 2
- skip_gain: float32 [8], replicated, may hold values from 0.1 to 1.9
- out_gain: bfloat16 [512], P('tp'), may hold values from 0.099609375 to 1.8984375
- proj_out: bfloat16 [512, 1024], P('tp'), may hold values from -0.25 to 0.25
- ffn_gain: bfloat16 [1024], replicated, may hold values from 0.099609375 to 1.8984375
- expert_ids: int32 [256, 6], P('ep'), may hold values from 0 to 15, all different within a row; in each aligned block of 16 rows (0 to 15, 16 to 31, ...) at most 9 rows name the same one
- expert_weights: float32 [256, 6], P('ep'), may hold values from 0.05 to 1
- expert_gate: bfloat16 [16, 1024, 512], P('ep', None, 'tp'), may hold values from -0.1875 to 0.1875
- expert_up: bfloat16 [16, 1024, 512], P('ep', None, 'tp'), may hold values from -0.1875 to 0.1875
- expert_down: bfloat16 [16, 512, 1024], P('ep', 'tp'), may hold values from -0.25 to 0.25
- dense_gate: bfloat16 [1024, 1024], P(None, 'tp'), may hold values from -0.1875 to 0.1875
- dense_up: bfloat16 [1024, 1024], P(None, 'tp'), may hold values from -0.1875 to 0.1875
- dense_down: bfloat16 [1024, 1024], P(None, 'tp'), may hold values from -0.5 to 0.5
- branch_gate: bfloat16 [1024], replicated, may hold values from -0.1875 to 0.1875
Outputs:
- new_hidden: bfloat16 [256, 1024], P('ep', 'tp')
- new_state: float32 [256, 8, 64, 64], P('ep', 'tp')
- new_input_window: bfloat16 [256, 3, 512], P('ep', None, 'tp')
- new_write_window: bfloat16 [256, 3, 256], P('ep', None, 'tp')
- new_read_window: bfloat16 [256, 3, 256], P('ep', None, 'tp')
Inputs may be any that keep to these rules, and one draw needn't show every extreme that they name: `expert_ids`: each row names 6 different experts. Among the 16 rows of one index of ep no expert is named more than 9 times, and in some aligned block an expert is named exactly 9 times.
All inputs are finite; a program needn't handle non-finite values.
Results may differ from a plain program's by a relative error of at most 0.018.
Values may be sent and summed in bfloat16 or wider, within the bound.
A program may use at most 64 MiB of HBM per device.

v0:
```python
import jax
import jax.numpy as jnp
from jax import lax
from jax.sharding import PartitionSpec as P

HEADS = 8
HEAD_DIM = 64
STATE = 64
BC_GROUPS = 4


EPS = 1e-06


def short_conv(window, newest, taps):
    stacked = jnp.concatenate([window, newest[:, None, :]], axis=1)
    mixed = jnp.sum(stacked.astype(jnp.float32) * taps.astype(jnp.float32)[None], axis=1)
    return (jax.nn.silu(mixed), stacked[:, 1:, :])


def local(
    tokens,
    input_window,
    write_window,
    read_window,
    ssm_state,
    norm_gain,
    proj_gate,
    proj_input,
    proj_write,
    proj_read,
    proj_step,
    taps_input,
    taps_write,
    taps_read,
    step_bias,
    decay_rate,
    skip_gain,
    out_gain,
    proj_out,
    ffn_gain,
    expert_ids,
    expert_weights,
    expert_gate,
    expert_up,
    expert_down,
    dense_gate,
    dense_up,
    dense_down,
    branch_gate,
):
    tp_rank = lax.axis_index("tp")
    ep_count = lax.axis_size("ep")
    row_count = tokens.shape[0]
    width = norm_gain.shape[0]
    quarter = tokens.shape[1]
    col_start = tp_rank * quarter
    widened = tokens.astype(jnp.float32)
    squares = lax.psum(jnp.sum(widened * widened, axis=1), "tp")
    gain_part = lax.dynamic_slice_in_dim(norm_gain, col_start, quarter, 0).astype(jnp.float32)
    normed_part = (widened * lax.rsqrt(squares / width + EPS)[:, None] * gain_part).astype(
        jnp.bfloat16
    )
    normed = lax.all_gather(normed_part, "tp", axis=1, tiled=True)
    heads_dev = proj_gate.shape[1] // HEAD_DIM
    head_start = tp_rank * heads_dev
    per_group = HEADS // BC_GROUPS
    groups_dev = heads_dev // per_group
    gate_rows = jnp.dot(normed, proj_gate, preferred_element_type=jnp.float32).astype(jnp.bfloat16)
    input_rows = jnp.dot(normed, proj_input, preferred_element_type=jnp.float32).astype(
        jnp.bfloat16
    )
    write_rows = jnp.dot(normed, proj_write, preferred_element_type=jnp.float32).astype(
        jnp.bfloat16
    )
    read_rows = jnp.dot(normed, proj_read, preferred_element_type=jnp.float32).astype(jnp.bfloat16)
    step_all = jnp.dot(normed, proj_step, preferred_element_type=jnp.float32)
    step_raw = lax.dynamic_slice_in_dim(step_all, head_start, heads_dev, 1)
    input_conv, new_input_window = short_conv(input_window, input_rows, taps_input)
    write_conv, new_write_window = short_conv(write_window, write_rows, taps_write)
    read_conv, new_read_window = short_conv(read_window, read_rows, taps_read)
    bias_part = lax.dynamic_slice_in_dim(step_bias, head_start, heads_dev, 0)
    rate_part = lax.dynamic_slice_in_dim(decay_rate, head_start, heads_dev, 0)
    skip_part = lax.dynamic_slice_in_dim(skip_gain, head_start, heads_dev, 0)
    step_size = jax.nn.softplus(step_raw + bias_part)
    decay = jnp.exp(-step_size * rate_part)
    heads_input = input_conv.reshape(row_count, heads_dev, HEAD_DIM)
    write_heads = jnp.repeat(write_conv.reshape(row_count, groups_dev, STATE), per_group, axis=1)
    read_heads = jnp.repeat(read_conv.reshape(row_count, groups_dev, STATE), per_group, axis=1)
    new_state = (
        decay[:, :, None, None] * ssm_state
        + (step_size[:, :, None] * heads_input)[:, :, :, None] * write_heads[:, :, None, :]
    )
    readout = jnp.einsum("bhpn,bhn->bhp", new_state, read_heads, precision=lax.Precision.HIGHEST)
    readout = readout + skip_part[None, :, None] * heads_input
    gated = readout.reshape(row_count, heads_dev * HEAD_DIM) * jax.nn.silu(
        gate_rows.astype(jnp.float32)
    )
    grouped = gated.reshape(row_count, groups_dev, -1)
    grouped = grouped * lax.rsqrt(jnp.mean(grouped * grouped, axis=-1, keepdims=True) + EPS)
    mixer_rows = (
        grouped.reshape(row_count, heads_dev * HEAD_DIM) * out_gain.astype(jnp.float32)
    ).astype(jnp.bfloat16)
    partial_value = jnp.dot(mixer_rows, proj_out, preferred_element_type=jnp.float32)
    mixed = lax.psum_scatter(
        partial_value.astype(jnp.bfloat16), "tp", scatter_dimension=1, tiled=True
    ).astype(jnp.float32)
    hidden_part = (tokens.astype(jnp.float32) + mixed).astype(jnp.bfloat16)
    hidden_wide = hidden_part.astype(jnp.float32)
    squares_ffn = lax.psum(jnp.sum(hidden_wide * hidden_wide, axis=1), "tp")
    ffn_part = lax.dynamic_slice_in_dim(ffn_gain, col_start, quarter, 0).astype(jnp.float32)
    normed_ffn_part = (
        hidden_wide * lax.rsqrt(squares_ffn / width + EPS)[:, None] * ffn_part
    ).astype(jnp.bfloat16)
    normed_ffn = lax.all_gather(normed_ffn_part, "tp", axis=1, tiled=True)
    local_experts = expert_gate.shape[0]
    expert_total = local_experts * ep_count
    top_count = expert_ids.shape[1]
    capacity = min(
        row_count, max(2, (3 * row_count * top_count + 2 * expert_total - 1) // (2 * expert_total))
    )
    slot_total = expert_total * capacity
    flat_ids = expert_ids.reshape(-1)
    hits = (flat_ids[:, None] == jnp.arange(expert_total, dtype=jnp.int32)[None, :]).astype(
        jnp.int32
    )
    before = jnp.cumsum(hits, axis=0) - hits
    place = jnp.sum(before * hits, axis=1)
    slots = (flat_ids * capacity + place).reshape(row_count, top_count)
    matches = slots[:, :, None] == jnp.arange(slot_total, dtype=jnp.int32)[None, None, :]
    chosen = jnp.any(matches, axis=1).astype(jnp.bfloat16)
    outgoing = jnp.einsum("rs,rd->sd", chosen, normed_ffn, preferred_element_type=jnp.float32)
    outgoing = outgoing.astype(jnp.bfloat16).reshape(expert_total, capacity, width)
    arrived = lax.all_to_all(outgoing, "ep", split_axis=0, concat_axis=0, tiled=True)
    item_count = arrived.shape[1]
    grouped_in = arrived.reshape(-1, local_experts, item_count, width)
    gate_part = jnp.einsum(
        "secd,edf->secf", grouped_in, expert_gate, preferred_element_type=jnp.float32
    )
    up_part = jnp.einsum(
        "secd,edf->secf", grouped_in, expert_up, preferred_element_type=jnp.float32
    )
    hidden = (jax.nn.silu(gate_part) * up_part).astype(jnp.bfloat16)
    partial_out = jnp.einsum(
        "secf,efd->secd", hidden, expert_down, preferred_element_type=jnp.float32
    )
    summed = lax.psum_scatter(
        partial_out.reshape(-1, item_count, width).astype(jnp.bfloat16),
        "tp",
        scatter_dimension=2,
        tiled=True,
    )
    returned = lax.all_to_all(summed, "ep", split_axis=0, concat_axis=0, tiled=True)
    weights_on = jnp.sum(jnp.where(matches, expert_weights[:, :, None], 0.0), axis=1)
    expert_sum = jnp.dot(
        weights_on,
        returned.reshape(slot_total, quarter).astype(jnp.float32),
        precision=lax.Precision.HIGHEST,
    )
    dense_hidden = (
        jax.nn.silu(jnp.dot(normed_ffn, dense_gate, preferred_element_type=jnp.float32))
        * jnp.dot(normed_ffn, dense_up, preferred_element_type=jnp.float32)
    ).astype(jnp.bfloat16)
    dense_partial = lax.dot_general(
        dense_hidden, dense_down, (((1,), (1,)), ((), ())), preferred_element_type=jnp.float32
    )
    dense_sum = lax.psum_scatter(
        dense_partial.astype(jnp.bfloat16), "tp", scatter_dimension=1, tiled=True
    ).astype(jnp.float32)
    branch = jax.nn.sigmoid(jnp.dot(normed_ffn, branch_gate, preferred_element_type=jnp.float32))
    new_hidden = (
        hidden_part.astype(jnp.float32) + expert_sum + branch[:, None] * dense_sum
    ).astype(jnp.bfloat16)
    return (new_hidden, new_state, new_input_window, new_write_window, new_read_window)


def solution(mesh):
    in_specs = (
        P("ep", "tp"),
        P("ep", None, "tp"),
        P("ep", None, "tp"),
        P("ep", None, "tp"),
        P("ep", "tp", None, None),
        P(),
        P(None, "tp"),
        P(None, "tp"),
        P(None, "tp"),
        P(None, "tp"),
        P(),
        P(None, "tp"),
        P(None, "tp"),
        P(None, "tp"),
        P(),
        P(),
        P(),
        P("tp"),
        P("tp", None),
        P(),
        P("ep", None),
        P("ep", None),
        P("ep", None, "tp"),
        P("ep", None, "tp"),
        P("ep", "tp", None),
        P(None, "tp"),
        P(None, "tp"),
        P(None, "tp"),
        P(),
    )
    out_specs = (
        P("ep", "tp"),
        P("ep", "tp", None, None),
        P("ep", None, "tp"),
        P("ep", None, "tp"),
        P("ep", None, "tp"),
    )
    return jax.shard_map(local, mesh=mesh, in_specs=in_specs, out_specs=out_specs, check_vma=False)
```

profile of v0, /device:TPU:0, one launch (start us, length us, event | category | flops | bytes accessed | tf_op | source)
XLA Modules:
  0.0 126.8 jit_solution(10707638776483695454)
XLA Ops:
  7.2 0.9 fusion.20
  8.1 5.9 %psum.14 = f32[16]{0:T(128)S(1)} all-reduce(f32[16]{0:T(128)S(1)} %fusion.20), channel_id=1, replica_groups=mesh['ep'=16,'tp'=2] {'tp'}, use_global_device_ids=true, to_apply=%region_1.0 | all-reduce | flops 16 | bytes 128 | tf_op jit(solution)/shard_map/psum | solution.py:59
  14.0 0.8 dynamic-slice_convert_fusion.1
  14.8 0.8 fusion.22
  15.6 4.4 %all_gather.6 = bf16[16,1024]{1,0:T(8,128)(2,1)S(1)} all-gather(bf16[16,512]{1,0:T(8,128)(2,1)S(1)} %fusion.22), channel_id=1, replica_groups=mesh['ep'=16,'tp'=2] {'tp'}, dimensions={1}, use_global_device_ids=true | all-gather | bytes 49152 | tf_op jit(solution)/shard_map/all_gather | solution.py:64
  20.0 0.7 convert_element_type.102
  20.6 1.1 fusion.8
  21.7 0.7 multiply_reduce_fusion.2
  22.6 0.7 dynamic_slice.21
  23.3 0.7 dynamic_slice.20
  24.0 0.8 fusion.42
  25.1 1.2 fusion.7
  26.3 0.7 convert_element_type.99
  27.0 0.7 multiply_reduce_fusion
  27.9 1.1 fusion.9
  29.0 0.7 convert_element_type.105
  29.7 0.7 multiply_reduce_fusion.1
  30.5 0.7 dynamic_slice.22
  31.4 2.0 %multiply_add_fusion = f32[16,4,64,64]{3,2,1,0:T(8,128)S(1)} fusion(f32[16,4,64,64]{3,2,1,0:T(8,128)} %param.33, f32[16,4,64]{2,1,0:T(4,128)S(1)} %bitcast.91, f32[16,4,64]{2,1,0:T(4,128)S(1)} %broadcast_multiply_fusion, f32[16,4]{1,0:T(8,128)S(1)} %copy.62), kind=kLoop, calls=%fused_computation | loop fusion | flops 786432 | bytes 2130176 | tf_op jit(solution)/shard_map/add | solution.py:91
  33.5 3.3 %fusion.43 = f32[16,4,1,64]{3,2,1,0:T(1,128)S(1)} fusion(f32[16,4,64,64]{3,2,1,0:T(8,128)S(1)} %multiply_add_fusion, f32[16,4,64,1]{2,3,1,0:T(1,128)S(1)} %bitcast.92), kind=kOutput, calls=%fused_computation.92 | convolution fusion | flops 3145728 | bytes 1081344 | tf_op jit(solution)/shard_map/bhpn,bhn->bhp/dot_general | solution.py:94
  37.0 1.2 fusion.41
  38.5 1.8 %convolution_convert_fusion.3 = bf16[16,1024]{1,0:T(8,128)(2,1)} fusion(bf16[256,1024]{1,0:T(8,128)(2,1)} %param.47, f32[16,256]{1,0:T(8,128)S(1)} %get-tuple-element.8, f32[2,8,2,128]{3,2,1,0:T(2,128)S(1)} %bitcast.93, f32[256]{0:T(256)S(1)} %convert_element_type.108), kind=kOutput, calls=%fused_computation.9 | convolution fusion | flops 8417280 | bytes 590848 | tf_op jit(solution)/shard_map/dot_general | solution.py:104
  40.6 0.1 reduce_window_sum.11
  40.7 0.2 select_reduce_fusion.1
  41.1 0.1 fusion.17
  41.3 10.9 %reduce-scatter.4.cloned.1.call-done = bf16[16,512]{1,0:T(8,128)(2,1)} async-done(((bf16[16,1024]{1,0:T(8,128)(2,1)}), bf16[16,512]{1,0:T(8,128)(2,1)}) %reduce-scatter.4.cloned.1.call-update) | async-done | bytes 16400 | tf_op jit(solution)/shard_map/reduce_scatter | solution.py:105
  52.2 0.8 fusion.24
  53.1 4.9 %psum.15 = f32[16]{0:T(128)S(1)} all-reduce(f32[16]{0:T(128)S(1)} %fusion.24), channel_id=1, replica_groups=mesh['ep'=16,'tp'=2] {'tp'}, use_global_device_ids=true, to_apply=%region_12.13 | all-reduce | flops 16 | bytes 128 | tf_op jit(solution)/shard_map/psum | solution.py:110
  58.0 0.8 fusion.26
  58.8 4.4 %all_gather.7 = bf16[16,1024]{1,0:T(8,128)(2,1)S(1)} all-gather(bf16[16,512]{1,0:T(8,128)(2,1)S(1)} %fusion.26), channel_id=1, replica_groups=mesh['ep'=16,'tp'=2] {'tp'}, dimensions={1}, use_global_device_ids=true | all-gather | bytes 49152 | tf_op jit(solution)/shard_map/all_gather | solution.py:115
  63.2 0.3 convolution_convert_fusion
  63.5 0.9 reshape.100
  64.4 5.7 %all-to-all-start = ((bf16[16,9,1024]{2,1,0:T(8,128)(2,1)}), bf16[16,9,1024]{2,1,0:T(8,128)(2,1)S(1)}, u32[]{:S(2)}, u32[]{:S(2)}) async-start(bf16[16,9,1024]{2,1,0:T(8,128)(2,1)} %reshape.100), calls=%async_computation.1 | async-start | bytes 1048576 | tf_op jit(solution)/shard_map/all_to_all | solution.py:134
  70.3 14.2 %all-to-all-done = bf16[16,9,1024]{2,1,0:T(8,128)(2,1)S(1)} async-done(((bf16[16,9,1024]{2,1,0:T(8,128)(2,1)}), bf16[16,9,1024]{2,1,0:T(8,128)(2,1)S(1)}, u32[]{:S(2)}, u32[]{:S(2)}) %all-to-all-start) | async-done | bytes 294944 | tf_op jit(solution)/shard_map/all_to_all | solution.py:134
  84.4 1.4 %convolution_bitcast_fusion.1 = f32[16,1,9,256]{3,2,0,1:T(8,128)S(1)} fusion(bf16[16,9,1024]{2,1,0:T(8,128)(2,1)S(1)} %all-to-all-done, bf16[1,1024,256]{2,1,0:T(8,128)(2,1)} %param.51), kind=kOutput, calls=%fused_computation.5 | convolution fusion | flops 75497472 | bytes 966656 | tf_op jit(solution)/shard_map/secd,edf->secf/dot_general | solution.py:137
  85.9 0.3 fusion.2
  86.2 1.0 convolution_convert_fusion.1
  87.2 0.6 fusion.32
  87.8 0.6 fusion.36
  88.5 0.2 fusion.44
  88.8 9.3 %reduce-scatter.6.cloned.1.call-done = bf16[16,9,512]{2,0,1:T(8,128)(2,1)} async-done(((bf16[16,9,1024]{2,0,1:T(8,128)(2,1)}), bf16[16,9,512]{2,0,1:T(8,128)(2,1)}) %reduce-scatter.6.cloned.1.call-update) | async-done | bytes 147472 | tf_op jit(solution)/shard_map/reduce_scatter | solution.py:147
  98.1 1.7 %copy.67 = bf16[16,9,512]{2,1,0:T(8,128)(2,1)} copy(bf16[16,9,512]{2,0,1:T(8,128)(2,1)} %reduce-scatter.6.cloned.1.call-done) | data formatting | bytes 294912 | tf_op jit(solution)/shard_map/reduce_scatter | solution.py:147
  99.8 5.6 %all-to-all-start.1 = ((bf16[16,9,512]{2,1,0:T(8,128)(2,1)}), bf16[16,9,512]{2,1,0:T(8,128)(2,1)S(1)}, u32[]{:S(2)}, u32[]{:S(2)}) async-start(bf16[16,9,512]{2,1,0:T(8,128)(2,1)} %copy.67), calls=%async_computation.3 | async-start | bytes 524288 | tf_op jit(solution)/shard_map/all_to_all | solution.py:153
  105.5 1.2 convolution_convert_fusion.2
  106.7 0.1 fusion.13
  106.8 8.6 %all-to-all-done.1 = bf16[16,9,512]{2,1,0:T(8,128)(2,1)S(1)} async-done(((bf16[16,9,512]{2,1,0:T(8,128)(2,1)}), bf16[16,9,512]{2,1,0:T(8,128)(2,1)S(1)}, u32[]{:S(2)}, u32[]{:S(2)}) %all-to-all-start.1) | async-done | bytes 147488 | tf_op jit(solution)/shard_map/all_to_all | solution.py:153
  115.5 3.3 %reduce-scatter.8.cloned.1.call-done = bf16[16,512]{1,0:T(8,128)(2,1)} async-done(((bf16[16,1024]{1,0:T(8,128)(2,1)}), bf16[16,512]{1,0:T(8,128)(2,1)}) %reduce-scatter.8.cloned.1.call-update) | async-done | bytes 16400 | tf_op jit(solution)/shard_map/reduce_scatter | solution.py:167
  118.8 1.5 %fusion.4 = bf16[16,512]{1,0:T(8,128)(2,1)} fusion(f32[16,144]{1,0:T(8,128)S(1)} %select_reduce_fusion, bf16[144,512]{1,0:T(8,128)(2,1)S(1)} %reshape.105, bf16[16,512]{1,0:T(8,128)(2,1)} %reduce-scatter.8.cloned.1.call-done, f32[16]{0:T(128)S(1)} %fusion.13, bf16[16,512]{1,0:T(8,128)(2,1)S(1)} %copy-done.6, bf16[16,512]{1,0:T(8,128)(2,1)S(1)} %copy-done.5), kind=kOutput, calls=%fused_computation.13 | convolution fusion | flops 14237696 | bytes 222272 | tf_op jit(solution)/shard_map/dot_general | solution.py:155
  (68 shorter events, 2.0 us)
Async XLA Ops:
  7.2 98.3 %copy-start = (bf16[1024,512]{1,0:T(8,128)(2,1)S(1)}, bf16[1024,512]{1,0:T(8,128)(2,1)}, u32[]{:S(2)}) copy-start(bf16[1024,512]{1,0:T(8,128)(2,1)} %param.56) | copy-start | bytes 3145732
  7.2 45.1 %reduce-scatter.4.cloned.1.call-start = ((), (), s32[]{:S(2)}) async-start(), calls=%async_computation.5 | async-start | bytes 49152 | tf_op jit(solution)/shard_map/reduce_scatter | solution.py:105
  33.4 30.1 %copy-start.1 = (f32[16,4,64,64]{3,2,1,0:T(8,128)}, f32[16,4,64,64]{3,2,1,0:T(8,128)S(1)}, u32[]{:S(2)}) copy-start(f32[16,4,64,64]{3,2,1,0:T(8,128)S(1)} %multiply_add_fusion) | copy-start | bytes 3145732
  33.4 5.0 %copy-start.15 = (bf16[256]{0:T(256)(128)(2,1)S(1)}, bf16[256]{0:T(256)(128)(2,1)}, u32[]{:S(2)}) copy-start(bf16[256]{0:T(256)(128)(2,1)} %param.46) | copy-start | bytes 1540
  33.4 6.9 %copy-start.10 = (s32[16,6]{0,1:T(8,128)S(1)}, s32[16,6]{0,1:T(8,128)}, u32[]{:S(2)}) copy-start(s32[16,6]{0,1:T(8,128)} %param.49) | copy-start | bytes 1156
  33.4 7.8 %copy-start.13 = (bf16[1024]{0:T(1024)(128)(2,1)S(1)}, bf16[1024]{0:T(1024)(128)(2,1)}, u32[]{:S(2)}) copy-start(bf16[1024]{0:T(1024)(128)(2,1)} %param.48) | copy-start | bytes 6148
  33.4 18.8 %copy-start.5 = (bf16[16,512]{1,0:T(8,128)(2,1)S(1)}, bf16[16,512]{1,0:T(8,128)(2,1)}, u32[]{:S(2)}) copy-start(bf16[16,512]{1,0:T(8,128)(2,1)} %param.29) | copy-start | bytes 49156
  36.8 33.4 %copy-start.12 = (bf16[1024]{0:T(1024)(128)(2,1)S(1)}, bf16[1024]{0:T(1024)(128)(2,1)}, u32[]{:S(2)}) copy-start(bf16[1024]{0:T(1024)(128)(2,1)} %param.57) | copy-start | bytes 6148
  64.4 21.4 %copy-start.14 = (bf16[1,1024,256]{2,1,0:T(8,128)(2,1)S(1)}, bf16[1,1024,256]{2,1,0:T(8,128)(2,1)}, u32[]{:S(2)}) copy-start(bf16[1,1024,256]{2,1,0:T(8,128)(2,1)} %param.52) | copy-start | bytes 1572868
  64.4 20.0 %all-to-all-start = ((bf16[16,9,1024]{2,1,0:T(8,128)(2,1)}), bf16[16,9,1024]{2,1,0:T(8,128)(2,1)S(1)}, u32[]{:S(2)}, u32[]{:S(2)}) async-start(bf16[16,9,1024]{2,1,0:T(8,128)(2,1)} %reshape.100), calls=%async_computation.1 | async-start | bytes 1048576 | tf_op jit(solution)/shard_map/all_to_all | solution.py:134
  70.2 27.9 %reduce-scatter.6.cloned.1.call-start = ((), (), s32[]{:S(2)}) async-start(), calls=%async_computation.6 | async-start | bytes 442368 | tf_op jit(solution)/shard_map/reduce_scatter | solution.py:147
  70.2 17.0 %copy-start.7 = (bf16[16,3,256]{2,0,1:T(8,128)(2,1)S(1)}, bf16[16,3,256]{2,0,1:T(8,128)(2,1)}, u32[]{:S(2)}) copy-start(bf16[16,3,256]{2,0,1:T(8,128)(2,1)} %param.30) | copy-start | bytes 73732
  70.2 17.6 %copy-start.8 = (bf16[16,3,128]{2,0,1:T(8,128)(2,1)S(1)}, bf16[16,3,128]{2,0,1:T(8,128)(2,1)}, u32[]{:S(2)}) copy-start(bf16[16,3,128]{2,0,1:T(8,128)(2,1)} %param.31) | copy-start | bytes 36868
  70.3 17.6 %copy-start.9 = (bf16[16,3,128]{2,0,1:T(8,128)(2,1)S(1)}, bf16[16,3,128]{2,0,1:T(8,128)(2,1)}, u32[]{:S(2)}) copy-start(bf16[16,3,128]{2,0,1:T(8,128)(2,1)} %param.32) | copy-start | bytes 36868
  84.4 1.8 %copy-start.4 = (bf16[1,256,1024]{2,1,0:T(8,128)(2,1)S(1)}, bf16[1,256,1024]{2,1,0:T(8,128)(2,1)}, u32[]{:S(2)}) copy-start(bf16[1,256,1024]{2,1,0:T(8,128)(2,1)} %param.53) | copy-start | bytes 1572868
  85.8 2.6 %copy-start.11 = (f32[16,6]{0,1:T(8,128)S(1)}, f32[16,6]{0,1:T(8,128)}, u32[]{:S(2)}) copy-start(f32[16,6]{0,1:T(8,128)} %param.50) | copy-start | bytes 1156
  85.9 2.7 %copy-start.2 = (bf16[1024,512]{1,0:T(8,128)(2,1)S(1)}, bf16[1024,512]{1,0:T(8,128)(2,1)}, u32[]{:S(2)}) copy-start(bf16[1024,512]{1,0:T(8,128)(2,1)} %param.54) | copy-start | bytes 3145732
  86.2 19.3 %copy-start.3 = (bf16[1024,512]{1,0:T(8,128)(2,1)S(1)}, bf16[1024,512]{1,0:T(8,128)(2,1)}, u32[]{:S(2)}) copy-start(bf16[1024,512]{1,0:T(8,128)(2,1)} %param.55) | copy-start | bytes 3145732
  88.5 30.2 %copy-start.6 = (bf16[16,512]{1,0:T(8,128)(2,1)S(1)}, bf16[16,512]{1,0:T(8,128)(2,1)}, u32[]{:S(2)}) copy-start(bf16[16,512]{1,0:T(8,128)(2,1)} %reduce-scatter.4.cloned.1.call-done) | copy-start | bytes 49156
  99.8 15.6 %all-to-all-start.1 = ((bf16[16,9,512]{2,1,0:T(8,128)(2,1)}), bf16[16,9,512]{2,1,0:T(8,128)(2,1)S(1)}, u32[]{:S(2)}, u32[]{:S(2)}) async-start(bf16[16,9,512]{2,1,0:T(8,128)(2,1)} %copy.67), calls=%async_computation.3 | async-start | bytes 524288 | tf_op jit(solution)/shard_map/all_to_all | solution.py:153
  105.4 13.4 %reduce-scatter.8.cloned.1.call-start = ((), (), s32[]{:S(2)}) async-start(), calls=%async_computation.7 | async-start | bytes 49152 | tf_op jit(solution)/shard_map/reduce_scatter | solution.py:167
Sparse Core Ops, SparseCore 0:
  40.5 11.7 reduce-scatter.3
  87.3 10.7 reduce-scatter.5
  108.4 10.3 reduce-scatter.7
where the time goes:
time: 128 us; the launch traced here: 127 us
  waiting for transfers between devices  46.3 us (36%)
  blocking collectives  19.6 us (15%)
  matrix products  16.7 us (13%)
  between operations  14.1 us (11%)
  other arithmetic  12.7 us (10%)
  starting transfers between devices  11.5 us (9%)
  local copies, waits for them, and re-layouts  5.93 us (5%)
    all_to_all x1, waiting for transfers between devices, local(): lax.all_to_all(outgoing, 'ep', split_axis=0, concat_axis=0, tiled=True)  14.2 us
    reduce_scatter x1, waiting for transfers between devices, local(): lax.psum_scatter(partial_value.astype(jnp.bfloat16), 'tp', scatter_dimens...  10.9 us
    reduce_scatter x1, waiting for transfers between devices, local(): lax.psum_scatter(partial_out.reshape(-1, item_count, width).astype(jnp.bf...  9.29 us
    all_to_all x1, waiting for transfers between devices, local(): lax.all_to_all(summed, 'ep', split_axis=0, concat_axis=0, tiled=True)  8.62 us
    psum x1, blocking collectives, local(): squares = lax.psum(jnp.sum(widened * widened, axis=1), 'tp')  5.86 us
    all_to_all x1, starting transfers between devices, local(): lax.all_to_all(outgoing, 'ep', split_axis=0, concat_axis=0, tiled=True)  5.74 us
    all_to_all x1, starting transfers between devices, local(): lax.all_to_all(summed, 'ep', split_axis=0, concat_axis=0, tiled=True)  5.62 us
    psum x1, blocking collectives, local(): squares_ffn = lax.psum(jnp.sum(hidden_wide * hidden_wide, axis=1), 'tp')  4.93 us
  transfers between devices with their start and end apart: 5, of which 5 were waited for; matrix products, arithmetic and copies ran while one was open for 3% of the time, Pallas kernels for 0%

commit v1 on v0

v1 whole, which is shorter than its diff:
```python
import functools

import jax
import jax.numpy as jnp
from jax import lax
from jax.experimental import pallas as pl
from jax.experimental.pallas import tpu as pltpu
from jax.sharding import PartitionSpec as P

HEADS = 8
HEAD_DIM = 64
STATE = 64
BC_GROUPS = 4
EPS = 1e-06
LANES = 8

F32 = jnp.float32
BF16 = jnp.bfloat16


def dot(a, b):
    return jnp.dot(a, b, preferred_element_type=F32)


def silu(v):
    return v / (1.0 + jnp.exp(-v))


def remote(src, dst, send, recv, where):
    return pltpu.make_async_remote_copy(
        src_ref=src,
        dst_ref=dst,
        send_sem=send,
        recv_sem=recv,
        device_id=where,
        device_id_type=pl.DeviceIdType.MESH,
    )


def drain(ref, sem):
    pltpu.make_async_copy(ref, ref, sem).wait()


def kernel(
    n_ep,
    n_tp,
    capacity,
    tokens,
    input_window,
    write_window,
    read_window,
    state_hbm,
    gains,
    proj_gate_hbm,
    proj_input_hbm,
    proj_write_hbm,
    proj_read_hbm,
    proj_step,
    taps_input,
    taps_write,
    taps_read,
    step_bias,
    decay_rate,
    skip_gain,
    proj_out_hbm,
    expert_ids,
    expert_weights,
    expert_gate_hbm,
    expert_up_hbm,
    expert_down_hbm,
    dense_gate_hbm,
    dense_up_hbm,
    dense_down_hbm,
    new_hidden,
    new_state_hbm,
    new_input_window,
    new_write_window,
    new_read_window,
    proj_gate,
    proj_input,
    proj_write,
    proj_read,
    proj_out,
    expert_gate,
    expert_up,
    expert_down,
    dense_gate,
    dense_up,
    dense_down,
    state,
    new_state,
    tok_all,
    part_all,
    hid_all,
    send_main,
    recv_main,
    send_extra,
    recv_extra,
    back_main,
    ret_main,
    back_extra,
    ret_extra,
    dense_send,
    dense_recv,
    weight_sems,
    state_sem,
    pair_send,
    pair_recv,
    a2a_send,
    a2a_recv,
):
    ep = lax.axis_index("ep")
    tp = lax.axis_index("tp")
    rows, quarter = tokens.shape
    width = quarter * n_tp
    main = capacity // LANES * LANES
    extra = capacity - main

    barrier = pltpu.get_barrier_semaphore()

    def greet(step, carry):
        for shift in range(n_tp):
            there = {"ep": lax.rem(ep + step, n_ep), "tp": lax.rem(tp + shift, n_tp)}

            def tell():
                pl.semaphore_signal(
                    barrier, inc=1, device_id=there, device_id_type=pl.DeviceIdType.MESH
                )

            if shift == 0:
                pl.when(step > 0)(tell)
            else:
                tell()
        return carry

    lax.fori_loop(0, n_ep, greet, 0)

    pairs = (
        (proj_gate_hbm, proj_gate),
        (proj_input_hbm, proj_input),
        (proj_write_hbm, proj_write),
        (proj_read_hbm, proj_read),
        (state_hbm, state),
        (proj_out_hbm, proj_out),
        (dense_gate_hbm, dense_gate),
        (dense_up_hbm, dense_up),
        (dense_down_hbm, dense_down),
        (expert_gate_hbm, expert_gate),
        (expert_up_hbm, expert_up),
        (expert_down_hbm, expert_down),
    )
    loads = [pltpu.make_async_copy(s, d, weight_sems.at[i]) for i, (s, d) in enumerate(pairs)]
    for load in loads:
        load.start()

    ids = expert_ids[...]
    weights = expert_weights[...]
    expert_lane = lax.broadcasted_iota(jnp.int32, (rows, n_ep), 1)
    hits = jnp.zeros((rows, n_ep), F32)
    scale = jnp.zeros((rows, n_ep), F32)
    for k in range(ids.shape[1]):
        same = ids[:, k : k + 1] == expert_lane
        hits = hits + jnp.where(same, 1.0, 0.0)
        scale = scale + jnp.where(same, weights[:, k : k + 1], 0.0)
    earlier = jnp.where(
        lax.broadcasted_iota(jnp.int32, (rows, rows), 1)
        < lax.broadcasted_iota(jnp.int32, (rows, rows), 0),
        1.0,
        0.0,
    ).astype(BF16)
    place = dot(earlier, hits.astype(BF16))
    scale_hi = scale.astype(BF16)
    scale_lo = (scale - scale_hi.astype(F32)).astype(BF16)
    if main:
        slots = n_ep * main
        slot = lax.broadcasted_iota(jnp.int32, (n_ep, slots), 1).astype(F32)
        owner = jnp.floor((slot + 0.5) / main)
        spread = jnp.where(
            owner == lax.broadcasted_iota(jnp.int32, (n_ep, slots), 0).astype(F32), 1.0, 0.0
        ).astype(BF16)
        lane = lax.broadcasted_iota(jnp.int32, (rows, slots), 1).astype(F32)
        index = lane - main * jnp.floor((lane + 0.5) / main)
        takes = jnp.logical_and(
            dot(hits.astype(BF16), spread) > 0.5, jnp.abs(dot(place.astype(BF16), spread) - index) < 0.5
        )
        chosen = jnp.where(takes, 1.0, 0.0)
        chosen_main = jnp.transpose(chosen).astype(BF16)
        main_hi = (dot(scale_hi, spread) * chosen).astype(BF16)
        main_lo = (dot(scale_lo, spread) * chosen).astype(BF16)
    chosen_extra, extra_hi, extra_lo = [], [], []
    for j in range(extra):
        takes = jnp.where(
            jnp.logical_and(hits > 0.5, jnp.abs(place - (main + j)) < 0.5), 1.0, 0.0
        )
        chosen_extra.append(takes.astype(BF16))
        extra_hi.append((scale_hi.astype(F32) * takes).astype(BF16))
        extra_lo.append((scale_lo.astype(F32) * takes).astype(BF16))

    pl.semaphore_wait(barrier, n_ep * n_tp - 1)

    def exchange(buffer, k):
        copies = []
        for shift in range(1, n_tp):
            copies.append(
                remote(
                    buffer.at[tp],
                    buffer.at[tp],
                    pair_send.at[k, shift],
                    pair_recv.at[k, shift],
                    {"tp": lax.rem(tp + shift, n_tp)},
                )
            )
            copies[-1].start()
        return copies

    tok_all[tp] = tokens[...]
    for copy in exchange(tok_all, 0):
        copy.wait()

    def norm(pieces, row):
        wide = jnp.concatenate(pieces, axis=1)
        factor = lax.rsqrt(jnp.sum(wide * wide, axis=1, keepdims=True) / width + EPS)
        return (wide * factor * gains[row : row + 1, :]).astype(BF16)

    token_parts = [tok_all[t].astype(F32) for t in range(n_tp)]
    normed = norm(token_parts, 0)

    for i in range(4):
        loads[i].wait()
    gate_rows = dot(normed, proj_gate[...]).astype(BF16)
    input_rows = dot(normed, proj_input[...]).astype(BF16)
    write_rows = dot(normed, proj_write[...]).astype(BF16)
    read_rows = dot(normed, proj_read[...]).astype(BF16)
    step_all = dot(normed, proj_step[...])

    def conv(window, newest, taps, result):
        old = window[...].astype(F32)
        lines = [old[:, i, :] for i in range(old.shape[1])] + [newest.astype(F32)]
        tap = taps[...].astype(F32)
        total = lines[0] * tap[0:1, :]
        for i in range(1, len(lines)):
            total = total + lines[i] * tap[i : i + 1, :]
        result[...] = jnp.stack(lines[1:], axis=1).astype(BF16)
        return silu(total)

    input_conv = conv(input_window, input_rows, taps_input, new_input_window)
    write_conv = conv(write_window, write_rows, taps_write, new_write_window)
    read_conv = conv(read_window, read_rows, taps_read, new_read_window)

    heads_dev = state.shape[1]
    groups_dev = write_conv.shape[1] // STATE
    per_group = heads_dev // groups_dev
    head_lane = lax.broadcasted_iota(jnp.int32, step_all.shape, 1)
    loads[4].wait()
    row_lane = lax.broadcasted_iota(jnp.int32, (HEAD_DIM, rows), 1)
    readouts = []
    for h in range(heads_dev):
        at = tp * heads_dev + h
        raw = jnp.sum(jnp.where(head_lane == at, step_all, 0.0), axis=1, keepdims=True)
        biased = raw + step_bias[at]
        size = jnp.maximum(biased, 0.0) + jnp.log1p(jnp.exp(-jnp.abs(biased)))
        decay = jnp.exp(-size * decay_rate[at])
        head_in = input_conv[:, h * HEAD_DIM : (h + 1) * HEAD_DIM]
        scaled = jnp.transpose(size * head_in)
        g = h // per_group
        write = write_conv[:, g * STATE : (g + 1) * STATE]
        read = read_conv[:, g * STATE : (g + 1) * STATE]
        columns = jnp.zeros((HEAD_DIM, rows), F32)
        for b in range(rows):
            fresh = decay[b : b + 1, :] * state[b, h] + scaled[:, b : b + 1] * write[b : b + 1, :]
            new_state[b, h] = fresh
            column = jnp.sum(fresh * read[b : b + 1, :], axis=1, keepdims=True)
            columns = jnp.where(row_lane == b, column, columns)
        readouts.append(jnp.transpose(columns) + skip_gain[at] * head_in)
    keep = pltpu.make_async_copy(new_state, new_state_hbm, state_sem)
    keep.start()
    gated = jnp.concatenate(readouts, axis=1) * silu(gate_rows.astype(F32))
    span = gated.shape[1] // groups_dev
    grouped = []
    for g in range(groups_dev):
        piece = gated[:, g * span : (g + 1) * span]
        grouped.append(
            piece * lax.rsqrt(jnp.mean(piece * piece, axis=1, keepdims=True) + EPS)
        )
    mixer_rows = (jnp.concatenate(grouped, axis=1) * gains[3:4, : gated.shape[1]]).astype(BF16)
    loads[5].wait()
    part_all[tp] = dot(mixer_rows, proj_out[...]).astype(BF16)
    for copy in exchange(part_all, 1):
        copy.wait()

    mixed = part_all[0].astype(F32)
    for t in range(1, n_tp):
        mixed = mixed + part_all[t].astype(F32)
    hidden_parts = []
    for t in range(n_tp):
        part = (token_parts[t] + mixed[:, t * quarter : (t + 1) * quarter]).astype(BF16)
        hid_all[t] = part
        hidden_parts.append(part.astype(F32))
    normed_ffn = norm(hidden_parts, 1)

    if main:
        send_main[...] = dot(chosen_main, normed_ffn).astype(BF16).reshape(send_main.shape)
    for j in range(extra):
        send_extra[j] = dot(jnp.transpose(chosen_extra[j].astype(F32)).astype(BF16), normed_ffn)[
            :, None, :
        ]

    def dispatch(step, carry):
        peer = lax.rem(ep + step, n_ep)
        if main:
            remote(
                send_main.at[peer], recv_main.at[ep], a2a_send.at[0], a2a_recv.at[0], {"ep": peer}
            ).start()
        for j in range(extra):
            remote(
                send_extra.at[j, peer],
                recv_extra.at[j, ep],
                a2a_send.at[1],
                a2a_recv.at[1],
                {"ep": peer},
            ).start()
        return carry

    lax.fori_loop(1, n_ep, dispatch, 0)
    if main:
        pltpu.make_async_copy(send_main.at[ep], recv_main.at[ep], a2a_recv.at[0]).start()
    for j in range(extra):
        pltpu.make_async_copy(send_extra.at[j, ep], recv_extra.at[j, ep], a2a_recv.at[1]).start()

    for i in range(6, 9):
        loads[i].wait()
    dense_hidden = (
        silu(dot(normed_ffn, dense_gate[...])) * dot(normed_ffn, dense_up[...])
    ).astype(BF16)
    for t in range(n_tp):
        dense_send[t] = lax.dot_general(
            dense_hidden,
            dense_down[t * quarter : (t + 1) * quarter, :],
            (((1,), (1,)), ((), ())),
            preferred_element_type=F32,
        ).astype(BF16)
    dense_copies = []
    for shift in range(1, n_tp):
        there = lax.rem(tp + shift, n_tp)
        dense_copies.append(
            remote(
                dense_send.at[there],
                dense_recv.at[tp],
                pair_send.at[2, shift],
                pair_recv.at[2, shift],
                {"tp": there},
            )
        )
        dense_copies[-1].start()
    logit = jnp.sum(normed_ffn.astype(F32) * gains[2:3, :], axis=1, keepdims=True)
    branch = 1.0 / (1.0 + jnp.exp(-logit))

    for i in range(9, 12):
        loads[i].wait()
    arrived = []
    if main:
        drain(recv_main, a2a_recv.at[0])
        arrived.append(recv_main[...].reshape(n_ep * main, width))
    if extra:
        drain(recv_extra, a2a_recv.at[1])
        for j in range(extra):
            arrived.append(recv_extra[j].reshape(n_ep, width).astype(BF16))
    arrived = jnp.concatenate(arrived, axis=0) if len(arrived) > 1 else arrived[0]
    hidden = (silu(dot(arrived, expert_gate[0])) * dot(arrived, expert_up[0])).astype(BF16)
    for t in range(n_tp):
        produced = dot(hidden, expert_down[0, :, t * quarter : (t + 1) * quarter])
        if main:
            back_main[t] = produced[: n_ep * main].astype(BF16).reshape(back_main.shape[1:])
        for j in range(extra):
            start = n_ep * (main + j)
            back_extra[j, t] = produced[start : start + n_ep][:, None, :]

    def give_back(step, carry):
        peer = lax.rem(ep + step, n_ep)
        for shift in range(n_tp):
            there = lax.rem(tp + shift, n_tp)

            def go():
                if main:
                    remote(
                        back_main.at[there, peer],
                        ret_main.at[tp, ep],
                        a2a_send.at[2],
                        a2a_recv.at[2],
                        {"ep": peer, "tp": there},
                    ).start()
                for j in range(extra):
                    remote(
                        back_extra.at[j, there, peer],
                        ret_extra.at[j, tp, ep],
                        a2a_send.at[3],
                        a2a_recv.at[3],
                        {"ep": peer, "tp": there},
                    ).start()

            if shift == 0:
                pl.when(step > 0)(go)
            else:
                go()
        return carry

    lax.fori_loop(0, n_ep, give_back, 0)
    if main:
        pltpu.make_async_copy(back_main.at[tp, ep], ret_main.at[tp, ep], a2a_recv.at[2]).start()
    for j in range(extra):
        pltpu.make_async_copy(
            back_extra.at[j, tp, ep], ret_extra.at[j, tp, ep], a2a_recv.at[3]
        ).start()

    for copy in dense_copies:
        copy.wait()
    dense_sum = dense_send[tp].astype(F32)
    for shift in range(1, n_tp):
        dense_sum = dense_sum + dense_recv[lax.rem(tp + shift, n_tp)].astype(F32)
    total = hid_all[tp].astype(F32) + branch * dense_sum

    if main:
        drain(ret_main, a2a_recv.at[2])
        for t in range(n_tp):
            back = ret_main[t].reshape(n_ep * main, quarter)
            total = total + dot(main_hi, back) + dot(main_lo, back)
    if extra:
        drain(ret_extra, a2a_recv.at[3])
        for j in range(extra):
            for t in range(n_tp):
                back = ret_extra[j, t].reshape(n_ep, quarter).astype(BF16)
                total = total + dot(extra_hi[j], back) + dot(extra_lo[j], back)
    new_hidden[...] = total.astype(BF16)

    def left(step, carry):
        if main:
            drain(send_main.at[0], a2a_send.at[0])
        for j in range(extra):
            drain(send_extra.at[j, 0], a2a_send.at[1])
        return carry

    lax.fori_loop(1, n_ep, left, 0)

    def left_back(step, carry):
        if main:
            drain(back_main.at[0, 0], a2a_send.at[2])
        for j in range(extra):
            drain(back_extra.at[j, 0, 0], a2a_send.at[3])
        return carry

    lax.fori_loop(1, n_ep * n_tp, left_back, 0)
    keep.wait()


def local(
    n_ep,
    n_tp,
    tokens,
    input_window,
    write_window,
    read_window,
    ssm_state,
    norm_gain,
    proj_gate,
    proj_input,
    proj_write,
    proj_read,
    proj_step,
    taps_input,
    taps_write,
    taps_read,
    step_bias,
    decay_rate,
    skip_gain,
    out_gain,
    proj_out,
    ffn_gain,
    expert_ids,
    expert_weights,
    expert_gate,
    expert_up,
    expert_down,
    dense_gate,
    dense_up,
    dense_down,
    branch_gate,
):
    rows, quarter = tokens.shape
    width = norm_gain.shape[0]
    top_count = expert_ids.shape[1]
    capacity = min(rows, max(2, (3 * rows * top_count + 2 * n_ep - 1) // (2 * n_ep)))
    main = capacity // LANES * LANES
    extra = capacity - main
    held = max(main, LANES)
    spare = max(extra, 1)
    gains = jnp.stack(
        [norm_gain, ffn_gain, branch_gate, jnp.pad(out_gain, (0, width - out_gain.shape[0]))]
    ).astype(F32)
    vmem = pl.BlockSpec(memory_space=pltpu.VMEM)
    smem = pl.BlockSpec(memory_space=pltpu.SMEM)
    hbm = pl.BlockSpec(memory_space=pl.ANY)
    streamed = (
        proj_gate,
        proj_input,
        proj_write,
        proj_read,
        proj_out,
        expert_gate,
        expert_up,
        expert_down,
        dense_gate,
        dense_up,
        dense_down,
        ssm_state,
    )
    shape_of = lambda a: jax.ShapeDtypeStruct(a.shape, a.dtype)
    return pl.pallas_call(
        functools.partial(kernel, n_ep, n_tp, capacity),
        out_shape=(
            shape_of(tokens),
            shape_of(ssm_state),
            shape_of(input_window),
            shape_of(write_window),
            shape_of(read_window),
        ),
        in_specs=[vmem] * 4
        + [hbm, vmem]
        + [hbm] * 4
        + [vmem] * 4
        + [smem] * 3
        + [hbm, vmem, vmem]
        + [hbm] * 6,
        out_specs=(vmem, hbm, vmem, vmem, vmem),
        scratch_shapes=[pltpu.VMEM(a.shape, a.dtype) for a in streamed]
        + [
            pltpu.VMEM(ssm_state.shape, F32),
            pltpu.VMEM((n_tp, rows, quarter), BF16),
            pltpu.VMEM((n_tp, rows, width), BF16),
            pltpu.VMEM((n_tp, rows, quarter), BF16),
            pltpu.VMEM((n_ep, held, width), BF16),
            pltpu.VMEM((n_ep, held, width), BF16),
            pltpu.VMEM((spare, n_ep, 1, width), F32),
            pltpu.VMEM((spare, n_ep, 1, width), F32),
            pltpu.VMEM((n_tp, n_ep, held, quarter), BF16),
            pltpu.VMEM((n_tp, n_ep, held, quarter), BF16),
            pltpu.VMEM((spare, n_tp, n_ep, 1, quarter), F32),
            pltpu.VMEM((spare, n_tp, n_ep, 1, quarter), F32),
            pltpu.VMEM((n_tp, rows, quarter), BF16),
            pltpu.VMEM((n_tp, rows, quarter), BF16),
            pltpu.SemaphoreType.DMA((12,)),
            pltpu.SemaphoreType.DMA,
            pltpu.SemaphoreType.DMA((3, n_tp)),
            pltpu.SemaphoreType.DMA((3, n_tp)),
            pltpu.SemaphoreType.DMA((4,)),
            pltpu.SemaphoreType.DMA((4,)),
        ],
        compiler_params=pltpu.CompilerParams(
            collective_id=0, has_side_effects=True, vmem_limit_bytes=60 * 1024 * 1024
        ),
    )(
        tokens,
        input_window,
        write_window,
        read_window,
        ssm_state,
        gains,
        proj_gate,
        proj_input,
        proj_write,
        proj_read,
        proj_step,
        taps_input,
        taps_write,
        taps_read,
        step_bias,
        decay_rate,
        skip_gain,
        proj_out,
        expert_ids,
        expert_weights,
        expert_gate,
        expert_up,
        expert_down,
        dense_gate,
        dense_up,
        dense_down,
    )


def solution(mesh):
    in_specs = (
        P("ep", "tp"),
        P("ep", None, "tp"),
        P("ep", None, "tp"),
        P("ep", None, "tp"),
        P("ep", "tp", None, None),
        P(),
        P(None, "tp"),
        P(None, "tp"),
        P(None, "tp"),
        P(None, "tp"),
        P(),
        P(None, "tp"),
        P(None, "tp"),
        P(None, "tp"),
        P(),
        P(),
        P(),
        P("tp"),
        P("tp", None),
        P(),
        P("ep", None),
        P("ep", None),
        P("ep", None, "tp"),
        P("ep", None, "tp"),
        P("ep", "tp", None),
        P(None, "tp"),
        P(None, "tp"),
        P(None, "tp"),
        P(),
    )
    out_specs = (
        P("ep", "tp"),
        P("ep", "tp", None, None),
        P("ep", None, "tp"),
        P("ep", None, "tp"),
        P("ep", None, "tp"),
    )
    step = functools.partial(local, mesh.shape["ep"], mesh.shape["tp"])
    return jax.shard_map(step, mesh=mesh, in_specs=in_specs, out_specs=out_specs, check_vma=False)
```

time: 128 us -> 60.1 us (0.47)
  the two profiles are of different devices: /device:TPU:0 before, /device:TPU:25 now
where the time goes in v1:
time: 60.1 us; the launch traced here: 59.3 us
  Pallas kernels  38.5 us (64%)
  local copies, waits for them, and re-layouts  19.5 us (32%)
  between operations  0.65 us (1%)
  other arithmetic  0.62 us (1%)
    pallas_call x1, Pallas kernels, local(): pl.pallas_call(functools.partial(kernel, n_ep, n_tp, capacity), out_shape...  38.5 us
    unnamed x8, local copies, waits for them, and re-layouts  12.8 us
    pallas_call x3, local copies, waits for them, and re-layouts, local(): pl.pallas_call(functools.partial(kernel, n_ep, n_tp, capacity), out_shape...  4.01 us
    another operation x4, local copies, waits for them, and re-layouts, local(): jnp.stack([norm_gain, ffn_gain, branch_gate, jnp.pad(out_gain, (0, width...  2.06 us

profile of v1, /device:TPU:25, one launch (start us, length us, event | category | flops | bytes accessed | tf_op | source)
XLA Modules:
  0.0 59.3 jit_solution(6797829150268658981)
XLA Ops:
  0.6 0.7 %pad.4 = bf16[1024]{0:T(1024)(128)(2,1)S(1)} pad(bf16[256]{0:T(256)(128)(2,1)} %param.46, bf16[]{:T(256)} %constant.2.clone.1), padding=0_768 | pad | bytes 2562 | tf_op jit(solution)/shard_map/jit(_pad)/pad | solution.py:497
  1.3 0.7 %stack.15 = bf16[1,1024]{1,0:T(2,128)(2,1)S(1)} reshape(bf16[1024]{0:T(1024)(128)(2,1)} %param.34) | data formatting | bytes 4096 | tf_op jit(solution)/shard_map/stack | solution.py:496
  2.0 0.7 %stack.16 = bf16[1,1024]{1,0:T(2,128)(2,1)S(1)} reshape(bf16[1024]{0:T(1024)(128)(2,1)} %param.48) | data formatting | bytes 4096 | tf_op jit(solution)/shard_map/stack | solution.py:496
  2.7 0.7 %stack.17 = bf16[1,1024]{1,0:T(2,128)(2,1)S(1)} reshape(bf16[1024]{0:T(1024)(128)(2,1)} %param.57) | data formatting | bytes 4096 | tf_op jit(solution)/shard_map/stack | solution.py:496
  3.4 0.6 %maximum_convert_fusion.gains = f32[4,1024]{1,0:T(4,128)} fusion(bf16[1,1024]{1,0:T(2,128)(2,1)S(1)} %stack.18, bf16[1,1024]{1,0:T(2,128)(2,1)S(1)} %stack.17, bf16[1,1024]{1,0:T(2,128)(2,1)S(1)} %stack.16, bf16[1,1024]{1,0:T(2,128)(2,1)S(1)} %stack.15), kind=kLoop, calls=%fused_computation | loop fusion | flops 32768 | bytes 24576 | tf_op jit(solution)/shard_map/convert_element_type | solution.py:498
  4.0 1.4 %copy.38.expert_ids = s32[16,6]{1,0:T(8,128)} copy(s32[16,6]{0,1:T(8,128)} %param.49) | data formatting | bytes 768 | tf_op args[20]
  5.3 1.4 %copy.39.expert_weights = f32[16,6]{1,0:T(8,128)} copy(f32[16,6]{0,1:T(8,128)} %param.50) | data formatting | bytes 768 | tf_op args[21]
  6.7 1.3 %copy.35.write_window = bf16[16,3,128]{2,1,0:T(4,128)(2,1)} copy(bf16[16,3,128]{2,0,1:T(8,128)(2,1)} %param.31) | data formatting | bytes 24576 | tf_op args[2]
  8.0 1.3 %copy.36.read_window = bf16[16,3,128]{2,1,0:T(4,128)(2,1)} copy(bf16[16,3,128]{2,0,1:T(8,128)(2,1)} %param.32) | data formatting | bytes 24576 | tf_op args[3]
  9.3 1.4 %copy.34.input_window = bf16[16,3,256]{2,1,0:T(4,128)(2,1)} copy(bf16[16,3,256]{2,0,1:T(8,128)(2,1)} %param.30) | data formatting | bytes 49152 | tf_op args[1]
  10.7 1.6 %copy.37.proj_step = bf16[1024,8]{1,0:T(8,128)(2,1)} copy(bf16[1024,8]{0,1:T(8,128)(2,1)} %param.39) | data formatting | bytes 32768 | tf_op args[10]
  12.3 38.5 %shard_map.308 = (bf16[16,512]{1,0:T(8,128)(2,1)}, f32[16,4,64,64]{3,2,1,0:T(8,128)}, bf16[16,3,256]{2,1,0:T(4,128)(2,1)}, bf16[16,3,128]{2,1,0:T(4,128)(2,1)}, bf16[16,3,128]{2,1,0:T(4,128)(2,1)}) custom-call(bf16[16,512]{1,0:T(8,128)(2,1)} %tokens.1, bf16[16,3,256]{2,1,0:T(4,128)(2,1)} %copy.34.input_window, bf16[16,3,128]{2,1,0:T(4,128)(2,1)} %copy.35.write_window, ...), custom_call_target="tpu_custom_call" | custom-call | tf_op jit(solution)/shard_map/pallas_call | solution.py:517
  50.8 1.3 %copy.41 = bf16[16,3,128]{2,0,1:T(8,128)(2,1)} copy(bf16[16,3,128]{2,1,0:T(4,128)(2,1)} %get-tuple-element.8) | data formatting | bytes 24576 | tf_op jit(solution)/shard_map/pallas_call | solution.py:517
  52.1 1.3 %copy.42 = bf16[16,3,128]{2,0,1:T(8,128)(2,1)} copy(bf16[16,3,128]{2,1,0:T(4,128)(2,1)} %get-tuple-element.9) | data formatting | bytes 24576 | tf_op jit(solution)/shard_map/pallas_call | solution.py:517
  53.4 1.4 %copy.40 = bf16[16,3,256]{2,0,1:T(8,128)(2,1)} copy(bf16[16,3,256]{2,1,0:T(4,128)(2,1)} %get-tuple-element.7) | data formatting | bytes 49152 | tf_op jit(solution)/shard_map/pallas_call | solution.py:517
  54.8 1.3 %copy.45 = bf16[16,512]{1,0:T(8,128)(2,1)} copy(bf16[16,512]{1,0:T(8,128)(2,1)} %get-tuple-element.15) | data formatting | bytes 32768
  56.1 3.2 %copy.46 = f32[16,4,64,64]{3,2,1,0:T(8,128)} copy(f32[16,4,64,64]{3,2,1,0:T(8,128)} %get-tuple-element.16) | data formatting | bytes 2097152
  (1 shorter events, 0.0 us)

commit v2 on v1

--- a/solution.py
+++ b/solution.py
@@ -13,6 +13,7 @@
 BC_GROUPS = 4
 EPS = 1e-06
 LANES = 8
+PIECES = 8
 
 F32 = jnp.float32
 BF16 = jnp.bfloat16
@@ -50,7 +51,10 @@
     write_window,
     read_window,
     state_hbm,
-    gains,
+    norm_gain,
+    ffn_gain,
+    branch_gate,
+    out_gain,
     proj_gate_hbm,
     proj_input_hbm,
     proj_write_hbm,
@@ -155,46 +159,47 @@
 
     ids = expert_ids[...]
     weights = expert_weights[...]
-    expert_lane = lax.broadcasted_iota(jnp.int32, (rows, n_ep), 1)
-    hits = jnp.zeros((rows, n_ep), F32)
-    scale = jnp.zeros((rows, n_ep), F32)
-    for k in range(ids.shape[1]):
-        same = ids[:, k : k + 1] == expert_lane
+    expert_row = lax.broadcasted_iota(jnp.int32, (n_ep, rows), 0)
+    hits = jnp.zeros((n_ep, rows), F32)
+    scale = jnp.zeros((n_ep, rows), F32)
+    for k in range(ids.shape[0]):
+        same = ids[k : k + 1, :] == expert_row
         hits = hits + jnp.where(same, 1.0, 0.0)
-        scale = scale + jnp.where(same, weights[:, k : k + 1], 0.0)
+        scale = scale + jnp.where(same, weights[k : k + 1, :], 0.0)
     earlier = jnp.where(
-        lax.broadcasted_iota(jnp.int32, (rows, rows), 1)
-        < lax.broadcasted_iota(jnp.int32, (rows, rows), 0),
+        lax.broadcasted_iota(jnp.int32, (rows, rows), 0)
+        < lax.broadcasted_iota(jnp.int32, (rows, rows), 1),
         1.0,
         0.0,
     ).astype(BF16)
-    place = dot(earlier, hits.astype(BF16))
+    place = dot(hits.astype(BF16), earlier)
     scale_hi = scale.astype(BF16)
     scale_lo = (scale - scale_hi.astype(F32)).astype(BF16)
     if main:
         slots = n_ep * main
-        slot = lax.broadcasted_iota(jnp.int32, (n_ep, slots), 1).astype(F32)
+        slot = lax.broadcasted_iota(jnp.int32, (slots, n_ep), 0).astype(F32)
         owner = jnp.floor((slot + 0.5) / main)
         spread = jnp.where(
-            owner == lax.broadcasted_iota(jnp.int32, (n_ep, slots), 0).astype(F32), 1.0, 0.0
+            owner == lax.broadcasted_iota(jnp.int32, (slots, n_ep), 1).astype(F32), 1.0, 0.0
         ).astype(BF16)
-        lane = lax.broadcasted_iota(jnp.int32, (rows, slots), 1).astype(F32)
+        lane = lax.broadcasted_iota(jnp.int32, (slots, rows), 0).astype(F32)
         index = lane - main * jnp.floor((lane + 0.5) / main)
         takes = jnp.logical_and(
-            dot(hits.astype(BF16), spread) > 0.5, jnp.abs(dot(place.astype(BF16), spread) - index) < 0.5
+            dot(spread, hits.astype(BF16)) > 0.5,
+            jnp.abs(dot(spread, place.astype(BF16)) - index) < 0.5,
         )
         chosen = jnp.where(takes, 1.0, 0.0)
-        chosen_main = jnp.transpose(chosen).astype(BF16)
-        main_hi = (dot(scale_hi, spread) * chosen).astype(BF16)
-        main_lo = (dot(scale_lo, spread) * chosen).astype(BF16)
+        chosen_main = chosen.astype(BF16)
+        main_hi = jnp.transpose(dot(spread, scale_hi) * chosen).astype(BF16)
+        main_lo = jnp.transpose(dot(spread, scale_lo) * chosen).astype(BF16)
     chosen_extra, extra_hi, extra_lo = [], [], []
     for j in range(extra):
         takes = jnp.where(
             jnp.logical_and(hits > 0.5, jnp.abs(place - (main + j)) < 0.5), 1.0, 0.0
         )
         chosen_extra.append(takes.astype(BF16))
-        extra_hi.append((scale_hi.astype(F32) * takes).astype(BF16))
-        extra_lo.append((scale_lo.astype(F32) * takes).astype(BF16))
+        extra_hi.append(jnp.transpose(scale_hi.astype(F32) * takes).astype(BF16))
+        extra_lo.append(jnp.transpose(scale_lo.astype(F32) * takes).astype(BF16))
 
     pl.semaphore_wait(barrier, n_ep * n_tp - 1)
 
@@ -217,13 +222,16 @@
     for copy in exchange(tok_all, 0):
         copy.wait()
 
-    def norm(pieces, row):
+    def as_row(gain):
+        return gain[...].astype(F32).reshape(1, gain.shape[0])
+
+    def norm(pieces, gain):
         wide = jnp.concatenate(pieces, axis=1)
         factor = lax.rsqrt(jnp.sum(wide * wide, axis=1, keepdims=True) / width + EPS)
-        return (wide * factor * gains[row : row + 1, :]).astype(BF16)
+        return (wide * factor * as_row(gain)).astype(BF16)
 
     token_parts = [tok_all[t].astype(F32) for t in range(n_tp)]
-    normed = norm(token_parts, 0)
+    normed = norm(token_parts, norm_gain)
 
     for i in range(4):
         loads[i].wait()
@@ -231,16 +239,19 @@
     input_rows = dot(normed, proj_input[...]).astype(BF16)
     write_rows = dot(normed, proj_write[...]).astype(BF16)
     read_rows = dot(normed, proj_read[...]).astype(BF16)
-    step_all = dot(normed, proj_step[...])
+    step_all = lax.dot_general(
+        normed, proj_step[...], (((1,), (1,)), ((), ())), preferred_element_type=F32
+    )
 
     def conv(window, newest, taps, result):
-        old = window[...].astype(F32)
-        lines = [old[:, i, :] for i in range(old.shape[1])] + [newest.astype(F32)]
+        old = [window[i] for i in range(window.shape[0])] + [newest]
+        lines = [line.astype(F32) for line in old]
         tap = taps[...].astype(F32)
         total = lines[0] * tap[0:1, :]
         for i in range(1, len(lines)):
             total = total + lines[i] * tap[i : i + 1, :]
-        result[...] = jnp.stack(lines[1:], axis=1).astype(BF16)
+        for i in range(1, len(lines)):
+            result[i - 1] = old[i]
         return silu(total)
 
     input_conv = conv(input_window, input_rows, taps_input, new_input_window)
@@ -282,7 +293,7 @@
         grouped.append(
             piece * lax.rsqrt(jnp.mean(piece * piece, axis=1, keepdims=True) + EPS)
         )
-    mixer_rows = (jnp.concatenate(grouped, axis=1) * gains[3:4, : gated.shape[1]]).astype(BF16)
+    mixer_rows = (jnp.concatenate(grouped, axis=1) * as_row(out_gain)).astype(BF16)
     loads[5].wait()
     part_all[tp] = dot(mixer_rows, proj_out[...]).astype(BF16)
     for copy in exchange(part_all, 1):
@@ -296,14 +307,12 @@
         part = (token_parts[t] + mixed[:, t * quarter : (t + 1) * quarter]).astype(BF16)
         hid_all[t] = part
         hidden_parts.append(part.astype(F32))
-    normed_ffn = norm(hidden_parts, 1)
+    normed_ffn = norm(hidden_parts, ffn_gain)
 
     if main:
         send_main[...] = dot(chosen_main, normed_ffn).astype(BF16).reshape(send_main.shape)
     for j in range(extra):
-        send_extra[j] = dot(jnp.transpose(chosen_extra[j].astype(F32)).astype(BF16), normed_ffn)[
-            :, None, :
-        ]
+        send_extra[j] = dot(chosen_extra[j], normed_ffn)[:, None, :]
 
     def dispatch(step, carry):
         peer = lax.rem(ep + step, n_ep)
@@ -352,7 +361,7 @@
             )
         )
         dense_copies[-1].start()
-    logit = jnp.sum(normed_ffn.astype(F32) * gains[2:3, :], axis=1, keepdims=True)
+    logit = jnp.sum(normed_ffn.astype(F32) * as_row(branch_gate), axis=1, keepdims=True)
     branch = 1.0 / (1.0 + jnp.exp(-logit))
 
     for i in range(9, 12):
@@ -450,6 +459,39 @@
 
     lax.fori_loop(1, n_ep * n_tp, left_back, 0)
     keep.wait()
+
+
+def hand_over(
+    hidden,
+    state,
+    input_window,
+    write_window,
+    read_window,
+    new_hidden,
+    new_state,
+    new_input_window,
+    new_write_window,
+    new_read_window,
+    held,
+    in_sems,
+    out_sems,
+):
+    size = held.shape[0] // PIECES
+    ins, outs = [], []
+    for i in range(PIECES):
+        piece = pl.ds(i * size, size)
+        ins.append(pltpu.make_async_copy(state.at[piece], held.at[piece], in_sems.at[i]))
+        outs.append(pltpu.make_async_copy(held.at[piece], new_state.at[piece], out_sems.at[i]))
+        ins[-1].start()
+    new_hidden[...] = hidden[...]
+    new_input_window[...] = input_window[...]
+    new_write_window[...] = write_window[...]
+    new_read_window[...] = read_window[...]
+    for i in range(PIECES):
+        ins[i].wait()
+        outs[i].start()
+    for copy in outs:
+        copy.wait()
 
 
 def local(
@@ -493,9 +535,6 @@
     extra = capacity - main
     held = max(main, LANES)
     spare = max(extra, 1)
-    gains = jnp.stack(
-        [norm_gain, ffn_gain, branch_gate, jnp.pad(out_gain, (0, width - out_gain.shape[0]))]
-    ).astype(F32)
     vmem = pl.BlockSpec(memory_space=pltpu.VMEM)
     smem = pl.BlockSpec(memory_space=pltpu.SMEM)
     hbm = pl.BlockSpec(memory_space=pl.ANY)
@@ -513,8 +552,11 @@
         dense_down,
         ssm_state,
     )
+    input_window = input_window.transpose(1, 0, 2)
+    write_window = write_window.transpose(1, 0, 2)
+    read_window = read_window.transpose(1, 0, 2)
     shape_of = lambda a: jax.ShapeDtypeStruct(a.shape, a.dtype)
-    return pl.pallas_call(
+    results = pl.pallas_call(
         functools.partial(kernel, n_ep, n_tp, capacity),
         out_shape=(
             shape_of(tokens),
@@ -524,7 +566,8 @@
             shape_of(read_window),
         ),
         in_specs=[vmem] * 4
-        + [hbm, vmem]
+        + [hbm]
+        + [vmem] * 4
         + [hbm] * 4
         + [vmem] * 4
         + [smem] * 3
@@ -563,12 +606,15 @@
         write_window,
         read_window,
         ssm_state,
-        gains,
+        norm_gain,
+        ffn_gain,
+        branch_gate,
+        out_gain,
         proj_gate,
         proj_input,
         proj_write,
         proj_read,
-        proj_step,
+        proj_step.T,
         taps_input,
         taps_write,
         taps_read,
@@ -576,14 +622,32 @@
         decay_rate,
         skip_gain,
         proj_out,
-        expert_ids,
-        expert_weights,
+        expert_ids.T,
+        expert_weights.T,
         expert_gate,
         expert_up,
         expert_down,
         dense_gate,
         dense_up,
         dense_down,
+    )
+    outputs = pl.pallas_call(
+        hand_over,
+        out_shape=tuple(shape_of(r) for r in results),
+        in_specs=[vmem, hbm, vmem, vmem, vmem],
+        out_specs=(vmem, hbm, vmem, vmem, vmem),
+        scratch_shapes=[
+            pltpu.VMEM(ssm_state.shape, F32),
+            pltpu.SemaphoreType.DMA((PIECES,)),
+            pltpu.SemaphoreType.DMA((PIECES,)),
+        ],
+    )(*results)
+    return (
+        outputs[0],
+        outputs[1],
+        outputs[2].transpose(1, 0, 2),
+        outputs[3].transpose(1, 0, 2),
+        outputs[4].transpose(1, 0, 2),
     )
 
 

time: 60.1 us -> 43.2 us (0.72)
  local copies, waits for them, and re-layouts: 19.5 us -> 0 us
  Pallas kernels: 38.5 us -> 42.3 us
  other arithmetic: 0.62 us -> 0 us
    unnamed x8 -> x0, local copies, waits for them, and re-layouts: 12.8 us -> none
    pallas_call x3 -> x0, local copies, waits for them, and re-layouts: 4.01 us -> none  [local(): pl.pallas_call(functools.partial(kernel, n_ep, n_tp, capacity), out_shape...]
    pallas_call x0 -> x1, Pallas kernels: none -> 3.77 us  [local(): pl.pallas_call(hand_over, out_shape=tuple((shape_of(r) for r in results))...]
    another operation x4 -> x0, local copies, waits for them, and re-layouts: 2.06 us -> none  [local(): jnp.stack([norm_gain, ffn_gain, branch_gate, jnp.pad(out_gain, (0, width...]
    pad x1 -> x0, local copies, waits for them, and re-layouts: 0.66 us -> none  [local(): jnp.pad(out_gain, (0, width - out_gain.shape[0]))]
    convert_element_type x1 -> x0, other arithmetic: 0.62 us -> none  [local(): gains = jnp.stack([norm_gain, ffn_gain, branch_gate, jnp.pad(out_gain, (0...]
where the time goes in v2:
time: 43.2 us; the launch traced here: 43 us
  Pallas kernels  42.3 us (98%)
  between operations  0.65 us (2%)
    pallas_call x1, Pallas kernels, local(): pl.pallas_call(functools.partial(kernel, n_ep, n_tp, capacity), out_shape...  38.5 us
    pallas_call x1, Pallas kernels, local(): pl.pallas_call(hand_over, out_shape=tuple((shape_of(r) for r in results))...  3.77 us

profile of v2, /device:TPU:25, one launch (start us, length us, event | category | flops | bytes accessed | tf_op | source)
XLA Modules:
  0.0 43.0 jit_solution(3304771715084484226)
XLA Ops:
  0.6 38.5 %shard_map.308 = (bf16[16,512]{1,0:T(8,128)(2,1)}, f32[16,4,64,64]{3,2,1,0:T(8,128)}, bf16[3,16,256]{2,1,0:T(8,128)(2,1)}, bf16[3,16,128]{2,1,0:T(8,128)(2,1)}, bf16[3,16,128]{2,1,0:T(8,128)(2,1)}) custom-call(bf16[16,512]{1,0:T(8,128)(2,1)} %tokens.1, bf16[3,16,256]{2,1,0:T(8,128)(2,1)} %bitcast.9, bf16[3,16,128]{2,1,0:T(8,128)(2,1)} %bitcast.11, ...), custom_call_target="tpu_custom_call" | custom-call | tf_op jit(solution)/shard_map/pallas_call | solution.py:559
  39.2 3.8 %shard_map.309 = (bf16[16,512]{1,0:T(8,128)(2,1)}, f32[16,4,64,64]{3,2,1,0:T(8,128)}, bf16[3,16,256]{2,1,0:T(8,128)(2,1)}, bf16[3,16,128]{2,1,0:T(8,128)(2,1)}, bf16[3,16,128]{2,1,0:T(8,128)(2,1)}) custom-call(bf16[16,512]{1,0:T(8,128)(2,1)} %get-tuple-element.15.hidden, f32[16,4,64,64]{3,2,1,0:T(8,128)} %get-tuple-element.16.state, ...), custom_call_target="tpu_custom_call" | custom-call | tf_op jit(solution)/shard_map/pallas_call | solution.py:634
